TPU v7x, 32 devices: a whole 2x2x4 slice. The times are simulated.
32 devices in a mesh: fs: 16 (over z, y, x), tp: 2 (over core).
Axes of the slice: x: 2, y: 2, z: 4, core: 2. Of those that a mesh axis runs over, the one named last changes fastest.
Arguments:
- tokens: bfloat16 [12288, 2048], P('fs'), may hold values from -6 to 6
- norm_gain: float32 [2048], replicated, may hold values from 0.1 to 1.9
- up_weight: float32 [2048, 8192], P('fs', 'tp'), may hold values from -0.125 to 0.125
- up_scale: float32 [8192], P('tp'), may hold values from 0.5 to 2
- down_weight: float32 [8192, 2048], P('tp', 'fs'), may hold values from -0.0625 to 0.0625
- down_scale: float32 [2048], P('fs'), may hold values from 0.5 to 2
Outputs:
- output: bfloat16 [12288, 2048], P('fs', 'tp')
All inputs are finite; a program needn't handle non-finite values.
Results may differ from a plain program's by a relative error of at most 0.015.
Values may be sent and summed in bfloat16 or wider, within the bound.
A program may use at most 128 MiB of HBM per device.

v0:
```python
import jax
import jax.numpy as jnp
from jax import lax
from jax.sharding import PartitionSpec as P

epsilon = 1e-06


def local(tokens, norm_gain, up_weight, up_scale, down_weight, down_scale):
    floats = tokens.astype(jnp.float32)
    inverse = lax.rsqrt(jnp.mean(floats * floats, axis=-1, keepdims=True) + epsilon)
    normed = (floats * inverse * norm_gain).astype(jnp.bfloat16)
    up_half = up_weight.astype(jnp.bfloat16)
    down_half = down_weight.astype(jnp.bfloat16)
    up_pre = jnp.dot(
        normed,
        lax.all_gather(up_half, "fs", axis=0, tiled=True),
        preferred_element_type=jnp.float32,
    )
    down_whole, scale_whole = (
        lax.all_gather(down_half, "fs", axis=1, tiled=True),
        lax.all_gather(down_scale.astype(jnp.bfloat16), "fs", axis=0, tiled=True).astype(
            down_scale.dtype
        ),
    )
    hidden = jnp.square(jax.nn.relu(up_pre * up_scale)).astype(jnp.bfloat16)
    partial_value = jnp.dot(hidden, down_whole, preferred_element_type=jnp.float32).astype(
        jnp.bfloat16
    )
    summed = lax.psum_scatter(
        partial_value.astype(jnp.float32).astype(jnp.bfloat16),
        "tp",
        scatter_dimension=1,
        tiled=True,
    ).astype(jnp.float32)
    own_width = summed.shape[1]
    own_scale = lax.dynamic_slice_in_dim(
        scale_whole, lax.axis_index("tp") * own_width, own_width, 0
    )
    return (summed * own_scale).astype(jnp.bfloat16)


def solution(mesh):
    in_specs = (P("fs", None), P(), P("fs", "tp"), P("tp"), P("tp", "fs"), P("fs"))
    out_specs = P("fs", "tp")
    return jax.shard_map(local, mesh=mesh, in_specs=in_specs, out_specs=out_specs, check_vma=False)
```

profile of v0, /device:TPU:0, one launch (start us, length us, event | category | flops | bytes accessed | tf_op | source)
XLA Modules:
  0.0 539.5 jit_solution(17070823121638339327)
XLA Ops:
  6.5 0.0 copy-start
  6.5 0.0 copy-start.1
  6.5 0.0 copy-start.2
  6.5 0.0 all-gather.6.cloned.1.call-start
  6.5 2.8 convert_element_type.36
  9.4 0.0 all-gather.6.cloned.1.call-update
  9.4 0.0 all-gather.4.cloned.1.call-start
  9.4 2.7 convert_element_type.34
  12.1 0.0 all-gather.4.cloned.1.call-update
  12.2 0.0 reduce-scatter.2.cloned.1.call-start
  12.2 0.0 copy-done
  12.2 0.7 fusion
  12.9 0.0 copy-start.3
  12.9 249.0 %all-gather.6.cloned.1.call-done = bf16[4096,2048]{1,0:T(8,128)(2,1)} async-done(((bf16[4096,128]{1,0:T(8,128)(2,1)}), bf16[4096,2048]{1,0:T(8,128)(2,1)}) %all-gather.6.cloned.1.call-update) | async-done | bytes 16777232 | tf_op jit(solution)/shard_map/all_gather | solution.py:21
  261.9 192.0 %all-gather.4.cloned.1.call-done = bf16[2048,4096]{1,0:T(8,128)(2,1)} async-done(((bf16[128,4096]{1,0:T(8,128)(2,1)}), bf16[2048,4096]{1,0:T(8,128)(2,1)}) %all-gather.4.cloned.1.call-update) | async-done | bytes 16777232 | tf_op jit(solution)/shard_map/all_gather | solution.py:17
  453.9 0.0 copy-done.1
  453.9 0.0 copy-done.2
  453.9 38.2 %convolution_convert_fusion = bf16[768,2048]{1,0:T(8,128)(2,1)} fusion(bf16[4096,2048]{1,0:T(8,128)(2,1)} %all-gather.6.cloned.1.call-done, bf16[2048,4096]{1,0:T(8,128)(2,1)} %all-gather.4.cloned.1.call-done, f32[4096]{0:T(1024)S(1)} %copy-done.1, bf16[768,2048]{1,0:T(8,128)(2,1)S(1)} %copy-done, f32[2048]{0:T(1024)S(1)} %copy-done.2, ...), kind=kOutput, calls=%fused_computation.6 | convolution fusion | flops 25790251008 | bytes 39873536 | tf_op jit(solution)/shard_map/dot_general | solution.py:27
  492.1 0.0 reduce-scatter.2.cloned.1.call-update
  492.2 0.0 copy-done.3
  492.2 37.8 %all-gather = bf16[16,1,128]{2,1,0:T(2,128)(2,1)S(1)} all-gather(bf16[1,1,128]{2,1,0:T(2,128)(2,1)S(1)} %convert_bitcast_fusion), channel_id=1, replica_groups=mesh['fs'=16,'tp'=2] {'fs'}, dimensions={0}, use_global_device_ids=true | all-gather | bytes 4352 | tf_op jit(solution)/shard_map/all_gather | solution.py:22
  530.0 0.0 reduce-scatter.2.cloned.1.call-done
  530.0 3.0 multiply_convert_fusion.1
  (4 shorter events, 0.0 us)
Async XLA Ops:
  6.5 5.7 %copy-start = (bf16[768,2048]{1,0:T(8,128)(2,1)S(1)}, bf16[768,2048]{1,0:T(8,128)(2,1)}, u32[]{:S(2)}) copy-start(bf16[768,2048]{1,0:T(8,128)(2,1)} %param.6) | copy-start | bytes 9437188
  6.5 447.4 %copy-start.1 = (f32[4096]{0:T(1024)S(1)}, f32[4096]{0:T(1024)}, u32[]{:S(2)}) copy-start(f32[4096]{0:T(1024)} %param.9) | copy-start | bytes 49156
  6.5 447.4 %copy-start.2 = (f32[2048]{0:T(1024)S(1)}, f32[2048]{0:T(1024)}, u32[]{:S(2)}) copy-start(f32[2048]{0:T(1024)} %param.7) | copy-start | bytes 24580
  6.5 255.4 %all-gather.6.cloned.1.call-start = ((), (), s32[]{:S(2)}) async-start(), calls=%async_computation.2 | async-start | bytes 17825792 | tf_op jit(solution)/shard_map/all_gather | solution.py:21
  9.4 444.5 %all-gather.4.cloned.1.call-start = ((), (), s32[]{:S(2)}) async-start(), calls=%async_computation.1 | async-start | bytes 17825792 | tf_op jit(solution)/shard_map/all_gather | solution.py:17
  12.2 517.9 %reduce-scatter.2.cloned.1.call-start = ((), (), s32[]{:S(2)}) async-start(), calls=%async_computation.3 | async-start | bytes 4718592 | tf_op jit(solution)/shard_map/reduce_scatter | solution.py:30
  12.9 479.3 %copy-start.3 = (f32[128]{0:T(128)S(1)}, f32[128]{0:T(128)}, u32[]{:S(2)}) copy-start(f32[128]{0:T(128)} %param.11) | copy-start | bytes 1540
Sparse Core Ops, SparseCore 0:
  10.0 251.8 all-gather.5
  264.7 189.1 all-gather.3
  492.3 9.1 reduce-scatter.1
where the time goes:
time: 540 us
  waiting for transfers between devices  441 us (82%)
  matrix products  38.2 us (7%)
  blocking collectives  37.8 us (7%)
  between operations  13.2 us (2%)
  other arithmetic  9.18 us (2%)
    all_gather x1, waiting for transfers between devices, local(): lax.all_gather(down_half, 'fs', axis=1, tiled=True)  249 us
    all_gather x1, waiting for transfers between devices, local(): lax.all_gather(up_half, 'fs', axis=0, tiled=True)  192 us
    dot_general x1, matrix products, local(): jnp.dot(hidden, down_whole, preferred_element_type=jnp.float32)  38.2 us
    all_gather x1, blocking collectives, local(): lax.all_gather(down_scale.astype(jnp.bfloat16), 'fs', axis=0, tiled=True)  37.8 us
  transfers between devices with their start and end apart: 3, of which 2 were waited for; matrix products, arithmetic and copies ran while one was open for 1% of the time, Pallas kernels for 0%

commit v1 on v0

--- a/solution.py
+++ b/solution.py
@@ -18,7 +18,9 @@
         preferred_element_type=jnp.float32,
     )
     down_whole, scale_whole = (
-        lax.all_gather(down_half, "fs", axis=1, tiled=True),
+        jnp.concatenate(
+            lax.all_to_all(jnp.stack([down_half] * lax.axis_size("fs")), "fs", 0, 0), axis=1
+        ),
         lax.all_gather(down_scale.astype(jnp.bfloat16), "fs", axis=0, tiled=True).astype(
             down_scale.dtype
         ),

time: 540 us -> 616 us (1.14)
  waiting for transfers between devices: 441 us -> 473 us
  blocking collectives: 37.8 us -> 67.6 us
  starting transfers between devices: 0.09 us -> 8.7 us
  local copies, waits for them, and re-layouts: 0.03 us -> 6.5 us
    all_gather x1, waiting for transfers between devices: 192 us -> 473 us  [local(): lax.all_gather(up_half, 'fs', axis=0, tiled=True)]
    all_gather x1 -> x0, waiting for transfers between devices: 249 us -> none  [local(): lax.all_gather(down_half, 'fs', axis=1, tiled=True)]
    all_gather x1, blocking collectives: 37.8 us -> 67.6 us  [local(): lax.all_gather(down_scale.astype(jnp.bfloat16), 'fs', axis=0, tiled=True)]
    dot_general x0 -> x1, matrix products: none -> 18.7 us  [local(): jnp.dot(normed, lax.all_gather(up_half, 'fs', axis=0, tiled=True), prefer...]
    dot_general x1, matrix products: 38.2 us -> 19.8 us  [local(): jnp.dot(hidden, down_whole, preferred_element_type=jnp.float32)]
    all_to_all x0 -> x1, starting transfers between devices: none -> 8.66 us  [local(): lax.all_to_all(jnp.stack([down_half] * lax.axis_size('fs')), 'fs', 0, 0)]
  transfers between devices with their start and end apart: 3 -> 3, of which waited for: 2 -> 1; matrix products, arithmetic and copies ran while one was open for 1% -> 4% of each run, Pallas kernels for 0% -> 0%
where the time goes in v1:
time: 616 us
  waiting for transfers between devices  473 us (77%)
  blocking collectives  67.6 us (11%)
  matrix products  38.4 us (6%)
  between operations  13.5 us (2%)
  starting transfers between devices  8.7 us (1%)
  other arithmetic  8.05 us (1%)
  local copies, waits for them, and re-layouts  6.5 us (1%)
    all_gather x1, waiting for transfers between devices, local(): lax.all_gather(up_half, 'fs', axis=0, tiled=True)  473 us
    all_gather x1, blocking collectives, local(): lax.all_gather(down_scale.astype(jnp.bfloat16), 'fs', axis=0, tiled=True)  67.6 us
    dot_general x1, matrix products, local(): jnp.dot(hidden, down_whole, preferred_element_type=jnp.float32)  19.8 us
    dot_general x1, matrix products, local(): jnp.dot(normed, lax.all_gather(up_half, 'fs', axis=0, tiled=True), prefer...  18.7 us
  transfers between devices with their start and end apart: 3, of which 1 were waited for; matrix products, arithmetic and copies ran while one was open for 4% of the time, Pallas kernels for 0%

profile of v1, /device:TPU:0, one launch (start us, length us, event | category | flops | bytes accessed | tf_op | source)
XLA Modules:
  0.0 615.9 jit_solution(33428019887355260)
XLA Ops:
  6.5 0.0 all-gather.3.cloned.1.call-start
  6.5 2.7 convert_element_type.34
  9.2 0.0 all-gather.3.cloned.1.call-update
  9.3 1.7 convert_element_type.36
  11.0 0.5 copy.8
  11.5 5.9 stack.2
  17.4 0.0 copy-start
  17.4 0.0 copy-start.1
  17.4 0.0 copy-start.2
  17.4 8.7 %all-to-all-start = ((bf16[16,4096,128]{1,2,0:T(8,128)(2,1)}), bf16[16,4096,128]{1,2,0:T(8,128)(2,1)}, u32[]{:S(2)}, u32[]{:S(2)}) async-start(bf16[16,4096,128]{1,2,0:T(8,128)(2,1)} %stack.2), calls=%async_computation | async-start | bytes 33554432 | tf_op jit(solution)/shard_map/all_to_all | solution.py:22
  26.1 0.0 reduce-scatter.2.cloned.1.call-start
  26.2 0.0 copy-done
  26.2 0.7 fusion
  26.9 473.1 %all-gather.3.cloned.1.call-done = bf16[2048,4096]{1,0:T(8,128)(2,1)} async-done(((bf16[128,4096]{1,0:T(8,128)(2,1)}), bf16[2048,4096]{1,0:T(8,128)(2,1)}) %all-gather.3.cloned.1.call-update) | async-done | bytes 16777232 | tf_op jit(solution)/shard_map/all_gather | solution.py:17
  500.0 0.0 copy-done.1
  500.0 0.0 copy-done.2
  500.0 18.7 %fusion.26 = bf16[768,4096]{1,0:T(8,128)(2,1)} fusion(f32[4096]{0:T(1024)S(1)} %copy-done.1, bf16[2048,4096]{1,0:T(8,128)(2,1)} %all-gather.3.cloned.1.call-done, bf16[768,2048]{1,0:T(8,128)(2,1)S(1)} %copy-done, f32[2048]{0:T(1024)S(1)} %copy-done.2, f32[768]{0:T(1024)S(1)} %add_rsqrt_fusion), kind=kOutput, calls=%bitcast_fusion.clone.1 | convolution fusion | flops 12903776256 | bytes 26242048 | tf_op jit(solution)/shard_map/dot_general | solution.py:15
  518.6 0.0 all-to-all-done
  518.6 0.0 copy-start.3
  518.6 19.8 %convolution_convert_fusion = bf16[768,2048]{1,0:T(8,128)(2,1)} fusion(bf16[4096,2048]{0,1:T(8,128)(2,1)} %bitcast.1, bf16[768,4096]{1,0:T(8,128)(2,1)} %fusion.26), kind=kOutput, calls=%fused_computation.6 | convolution fusion | flops 12886474752 | bytes 26214400 | tf_op jit(solution)/shard_map/dot_general | solution.py:29
  538.4 0.0 reduce-scatter.2.cloned.1.call-update
  538.4 0.0 copy-done.3
  538.4 67.6 %all-gather = bf16[16,1,128]{2,1,0:T(2,128)(2,1)S(1)} all-gather(bf16[1,1,128]{2,1,0:T(2,128)(2,1)S(1)} %convert_bitcast_fusion), channel_id=1, replica_groups=mesh['fs'=16,'tp'=2] {'fs'}, dimensions={0}, use_global_device_ids=true | all-gather | bytes 4352 | tf_op jit(solution)/shard_map/all_gather | solution.py:24
  606.1 0.0 reduce-scatter.2.cloned.1.call-done
  606.1 3.0 multiply_convert_fusion.1
  (4 shorter events, 0.0 us)
Async XLA Ops:
  6.5 493.4 %all-gather.3.cloned.1.call-start = ((), (), s32[]{:S(2)}) async-start(), calls=%async_computation.2 | async-start | bytes 17825792 | tf_op jit(solution)/shard_map/all_gather | solution.py:17
  17.4 8.7 %copy-start = (bf16[768,2048]{1,0:T(8,128)(2,1)S(1)}, bf16[768,2048]{1,0:T(8,128)(2,1)}, u32[]{:S(2)}) copy-start(bf16[768,2048]{1,0:T(8,128)(2,1)} %param.6) | copy-start | bytes 9437188
  17.4 482.5 %copy-start.1 = (f32[4096]{0:T(1024)S(1)}, f32[4096]{0:T(1024)}, u32[]{:S(2)}) copy-start(f32[4096]{0:T(1024)} %param.9) | copy-start | bytes 49156
  17.4 482.5 %copy-start.2 = (f32[2048]{0:T(1024)S(1)}, f32[2048]{0:T(1024)}, u32[]{:S(2)}) copy-start(f32[2048]{0:T(1024)} %param.7) | copy-start | bytes 24580
  17.4 501.2 %all-to-all-start = ((bf16[16,4096,128]{1,2,0:T(8,128)(2,1)}), bf16[16,4096,128]{1,2,0:T(8,128)(2,1)}, u32[]{:S(2)}, u32[]{:S(2)}) async-start(bf16[16,4096,128]{1,2,0:T(8,128)(2,1)} %stack.2), calls=%async_computation | async-start | bytes 33554432 | tf_op jit(solution)/shard_map/all_to_all | solution.py:22
  26.1 580.0 %reduce-scatter.2.cloned.1.call-start = ((), (), s32[]{:S(2)}) async-start(), calls=%async_computation.3 | async-start | bytes 4718592 | tf_op jit(solution)/shard_map/reduce_scatter | solution.py:32
  518.6 19.8 %copy-start.3 = (f32[128]{0:T(128)S(1)}, f32[128]{0:T(128)}, u32[]{:S(2)}) copy-start(f32[128]{0:T(128)} %param.11) | copy-start | bytes 1540
Sparse Core Ops, SparseCore 0:
  10.1 489.8 all-gather.2
  538.5 42.9 reduce-scatter.1
